TPU v7x, 32 devices: a whole 2x2x4 slice. The times are simulated.
32 devices in a mesh: ep: 16 (over z, y, x), tp: 2 (over core).
Axes of the slice: x: 2, y: 2, z: 4, core: 2. Of those that a mesh axis runs over, the one named last changes fastest.
Arguments:
- tokens: bfloat16 [256, 2048], P('ep'), may hold values from -6 to 6
- lengths: int32 [256], P('ep'), may hold values from 1 to 1024, as said below
- attn_gain: float32 [2048], replicated, may hold values from 0.1 to 1.9
- w_query: bfloat16 [2048, 1024], P(None, 'tp'), may hold values from -0.125 to 0.125
- w_key: bfloat16 [2048, 128], P(None, 'tp'), may hold values from -0.125 to 0.125
- w_value: bfloat16 [2048, 128], P(None, 'tp'), may hold values from -0.125 to 0.125
- head_bias: float32 [16], P('tp'), may hold values from -7 to -2
- key_cache: bfloat16 [256, 2, 64, 1024], P('ep', 'tp'), may hold values from -6 to 6
- value_cache: bfloat16 [256, 2, 64, 1024], P('ep', 'tp'), may hold values from -6 to 6
- w_attn_out: bfloat16 [1024, 2048], P('tp'), may hold values from -0.1875 to 0.1875
- ffn_gain: float32 [2048], replicated, may hold values from 0.1 to 1.9
- w_router: bfloat16 [2048, 16], replicated, may hold values from -0.125 to 0.125
- routes: int32 [256, 6], P('ep'), may hold values from 0 to 15, all different within a row; in each aligned block of 16 rows (0 to 15, 16 to 31, ...) at most 12 rows name the same one
- w_dense_gate: bfloat16 [2048, 512], P('ep', 'tp'), may hold values from -0.125 to 0.125
- w_dense_up: bfloat16 [2048, 512], P('ep', 'tp'), may hold values from -0.125 to 0.125
- w_dense_down: bfloat16 [512, 2048], P('tp', 'ep'), may hold values from -0.25 to 0.25
- dense_mix: float32 [2048], replicated, may hold values from -0.125 to 0.125
- w_expert_gate: bfloat16 [16, 2048, 512], P('ep', None, 'tp'), may hold values from -0.125 to 0.125
- w_expert_up: bfloat16 [16, 2048, 512], P('ep', None, 'tp'), may hold values from -0.125 to 0.125
- w_expert_down: bfloat16 [16, 512, 2048], P('ep', 'tp'), may hold values from -0.25 to 0.25
Outputs:
- layer_out: bfloat16 [256, 2048], P('ep', 'tp')
- new_keys: bfloat16 [256, 128], P('ep', 'tp')
- new_values: bfloat16 [256, 128], P('ep', 'tp')
Inputs may be any that keep to these rules, and one draw needn't show every extreme that they name: `lengths`: every sequence holds between 1 and 1024 cached positions; in every draw some sequence holds exactly 1024. `routes`: each token names 6 different experts. Among the rows of one device no expert is named by more than 12 rows.
All inputs are finite; a program needn't handle non-finite values.
Results may differ from a plain program's by a relative error of at most 0.014.
Values may be sent and summed in bfloat16 or wider, within the bound.
A program may use at most 64 MiB of HBM per device.

v0:
```python
import jax
import jax.numpy as jnp
from jax import lax
from jax.sharding import PartitionSpec as P


def rms_scale(values, gain):
    wide = values.astype(jnp.float32)
    return wide * lax.rsqrt(jnp.mean(wide * wide, axis=-1, keepdims=True) + 1e-06) * gain


def stick_read(queries, lengths, head_bias, key_cache, value_cache):
    seq_count, local_kv, head_dim, cache_len = key_cache.shape
    group_size = head_bias.shape[0] // local_kv
    grouped = queries.reshape(seq_count, local_kv, group_size, head_dim)
    head_shift = head_bias.reshape(1, local_kv, group_size, 1)
    span_len = min(512, cache_len)
    block_count = (jnp.max(lengths) + span_len - 1) // span_len
    span_index = lax.iota(jnp.int32, span_len)
    after_mask = (span_index[:, None] > span_index[None, :]).astype(jnp.float32)

    def visit(visit_index, carry):
        totals, log_later = carry
        first = (block_count - 1 - visit_index) * span_len
        key_block = lax.dynamic_slice_in_dim(key_cache, first, span_len, 3)
        value_block = lax.dynamic_slice_in_dim(value_cache, first, span_len, 3)
        scores = (
            jnp.einsum("skgd,skdc->skgc", grouped, key_block, preferred_element_type=jnp.float32)
            * head_dim ** (-0.5)
            + head_shift
        )
        positions = first + span_index
        visible = (positions[None, :] < lengths[:, None])[:, None, None, :]
        log_keep = jnp.where(visible, jax.nn.log_sigmoid(-scores), 0.0)
        log_after = (
            jnp.einsum("skgj,jc->skgc", log_keep, after_mask, precision=lax.Precision.HIGHEST)
            + log_later[..., None]
        )
        weights = jnp.where(visible, jnp.exp(jax.nn.log_sigmoid(scores) + log_after), 0.0).astype(
            jnp.bfloat16
        )
        totals = totals + jnp.einsum(
            "skgc,skdc->skgd", weights, value_block, preferred_element_type=jnp.float32
        )
        return (totals, log_later + jnp.sum(log_keep, axis=3))

    start_totals = jnp.zeros((seq_count, local_kv, group_size, head_dim), jnp.float32)
    start_later = jnp.zeros((seq_count, local_kv, group_size), jnp.float32)
    totals, unused_later = lax.fori_loop(0, block_count, visit, (start_totals, start_later))
    return totals.reshape(seq_count, -1).astype(jnp.bfloat16)


def expert_math(inputs, w_expert_gate, w_expert_up, w_expert_down):
    gate_rows = jnp.einsum(
        "njcd,jdf->njcf", inputs, w_expert_gate, preferred_element_type=jnp.float32
    )
    up_rows = jnp.einsum("njcd,jdf->njcf", inputs, w_expert_up, preferred_element_type=jnp.float32)
    hidden = (jax.nn.silu(gate_rows) * up_rows).astype(jnp.bfloat16)
    partial_value = jnp.einsum(
        "njcf,jfd->njcd", hidden, w_expert_down, preferred_element_type=jnp.float32
    ).astype(jnp.bfloat16)
    return (
        lax.psum_scatter(partial_value, "tp", scatter_dimension=3, tiled=True)
        .astype(jnp.float32)
        .astype(jnp.bfloat16)
    )


def shards(
    tokens,
    lengths,
    attn_gain,
    w_query,
    w_key,
    w_value,
    head_bias,
    key_cache,
    value_cache,
    w_attn_out,
    ffn_gain,
    w_router,
    routes,
    w_dense_gate,
    w_dense_up,
    w_dense_down,
    dense_mix,
    w_expert_gate,
    w_expert_up,
    w_expert_down,
):
    seq_count, model_width = tokens.shape
    normed = rms_scale(tokens, attn_gain).astype(jnp.bfloat16)
    new_keys = jnp.dot(normed, w_key, preferred_element_type=jnp.float32).astype(jnp.bfloat16)
    new_values = jnp.dot(normed, w_value, preferred_element_type=jnp.float32).astype(jnp.bfloat16)
    queries = jnp.dot(normed, w_query, preferred_element_type=jnp.float32).astype(jnp.bfloat16)
    heads_out = stick_read(queries, lengths, head_bias, key_cache, value_cache)
    attn_partial = jnp.dot(heads_out, w_attn_out, preferred_element_type=jnp.float32).astype(
        jnp.bfloat16
    )
    attn = lax.psum(attn_partial, "tp").astype(jnp.float32)
    residual = (tokens.astype(jnp.float32) + attn).astype(jnp.bfloat16)
    normed2 = rms_scale(residual, ffn_gain).astype(jnp.bfloat16)
    expert_total = w_router.shape[1]
    top_count = routes.shape[1]
    probs = jax.nn.sigmoid(jnp.dot(normed2, w_router, preferred_element_type=jnp.float32))
    hits = routes[:, :, None] == lax.iota(jnp.int32, expert_total)[None, None, :]
    picked = jnp.sum(jnp.where(hits, probs[:, None, :], 0.0), axis=-1)
    gates = picked / jnp.sum(picked, axis=-1, keepdims=True) * 2.5
    capacity = max(2, 2 * seq_count * top_count // expert_total)
    slot_total = expert_total * capacity
    flat_routes = routes.reshape(-1)
    route_count = flat_routes.shape[0]
    matching = flat_routes[:, None] == flat_routes[None, :]
    earlier = lax.iota(jnp.int32, route_count)[:, None] > lax.iota(jnp.int32, route_count)[None, :]
    slot_rank = jnp.sum(jnp.logical_and(matching, earlier).astype(jnp.int32), axis=1)
    target = flat_routes * capacity + slot_rank
    one_hot = (target[:, None] == lax.iota(jnp.int32, slot_total)[None, :]).astype(jnp.bfloat16)
    dispatch = jnp.sum(one_hot.reshape(seq_count, top_count, slot_total), axis=1)
    send_rows = jnp.einsum(
        "sr,sd->rd", dispatch, normed2, preferred_element_type=jnp.float32
    ).astype(jnp.bfloat16)
    send_rows = send_rows.reshape(expert_total, capacity, model_width)
    local_experts = w_expert_gate.shape[0]
    received = lax.all_to_all(send_rows, "ep", split_axis=0, concat_axis=0, tiled=True)
    source_count = received.shape[0] // local_experts
    item_count = received.shape[1]
    inputs = received.reshape(source_count, local_experts, item_count, model_width)
    summed = expert_math(inputs, w_expert_gate, w_expert_up, w_expert_down)
    summed = summed.reshape(source_count * local_experts, item_count, summed.shape[3])
    returned = lax.all_to_all(summed, "ep", split_axis=0, concat_axis=0, tiled=True)
    half_width = returned.shape[2]
    route_rows = returned.reshape(slot_total, half_width)[target]
    route_rows = route_rows.reshape(seq_count, top_count, half_width)
    routed = jnp.sum(gates[:, :, None] * route_rows.astype(jnp.float32), axis=1)
    features2 = lax.all_to_all(normed2, "ep", split_axis=1, concat_axis=0, tiled=True)
    paired_weights = jnp.concatenate([w_dense_gate, w_dense_up], axis=1)
    paired = lax.psum_scatter(
        jnp.dot(features2, paired_weights, preferred_element_type=jnp.float32),
        "ep",
        scatter_dimension=0,
        tiled=True,
    )
    hidden_cols = w_dense_gate.shape[1]
    dense_gate_rows = paired[:, :hidden_cols]
    dense_up_rows = paired[:, hidden_cols:]
    dense_hidden = (jax.nn.silu(dense_gate_rows) * dense_up_rows).astype(jnp.bfloat16)
    dense_columns = jnp.dot(
        lax.all_gather(dense_hidden, "ep", axis=0, tiled=True),
        w_dense_down,
        preferred_element_type=jnp.float32,
    )
    dense_partial = lax.all_to_all(
        dense_columns.astype(jnp.bfloat16), "ep", split_axis=0, concat_axis=1, tiled=True
    )
    dense = lax.psum_scatter(dense_partial, "tp", scatter_dimension=1, tiled=True).astype(
        jnp.float32
    )
    mix_gate = jax.nn.sigmoid(jnp.sum(normed2.astype(jnp.float32) * dense_mix, axis=-1))
    offset = lax.axis_index("tp") * half_width
    residual_half = lax.dynamic_slice_in_dim(residual, offset, half_width, 1)
    layer_out = (residual_half.astype(jnp.float32) + mix_gate[:, None] * dense + routed).astype(
        jnp.bfloat16
    )
    return (layer_out, new_keys, new_values)


def solution(mesh):
    return jax.shard_map(
        shards,
        mesh=mesh,
        in_specs=(
            P("ep", None),
            P("ep"),
            P(),
            P(None, "tp"),
            P(None, "tp"),
            P(None, "tp"),
            P("tp"),
            P("ep", "tp", None, None),
            P("ep", "tp", None, None),
            P("tp", None),
            P(),
            P(),
            P("ep", None),
            P("ep", "tp"),
            P("ep", "tp"),
            P("tp", "ep"),
            P(),
            P("ep", None, "tp"),
            P("ep", None, "tp"),
            P("ep", "tp", None),
        ),
        out_specs=(P("ep", "tp"), P("ep", "tp"), P("ep", "tp")),
        check_vma=False,
    )
```

profile of v0, /device:TPU:0, one launch (start us, length us, event | category | flops | bytes accessed | tf_op | source)
XLA Modules:
  0.0 217.0 jit_solution(16179048854171437925)
XLA Ops:
  7.2 1.4 reduce_max.9
  9.3 1.0 fusion.40
  10.3 2.1 convolution_convert_fusion.4
  12.5 3.9 %while.15 = (s32[]{:T(128)}, f32[16,1,8,64]{3,2,0,1:T(8,128)S(1)}, f32[16,1,8]{0,2,1:T(8,128)S(1)}, s32[]{:T(128)}, s32[]{:T(128)}, /*index=5*/s32[16]{0:T(128)S...) while((s32[]{:T(128)}, f32[16,1,8,64]{3,2,0,1:T(8,128)S(1)}, ...), condition=%wide.region_4.5_spmd.clone, body=%wide.region_2.4_spmd.clone.sunk | while | flops 422003200 | bytes 11420487 | solution.py:49
  12.7 1.6 fusion.88
  14.4 0.9 fusion.89
  15.3 0.7 copy-done.1
  16.6 1.0 convolution_convert_fusion.2
  18.3 23.8 %all-reduce.2.cloned.1.call-done = bf16[16,2048]{1,0:T(8,128)(2,1)} async-done(((bf16[16,2048]{1,0:T(8,128)(2,1)}), bf16[16,2048]{1,0:T(8,128)(2,1)}) %all-reduce.2.cloned.1.call-update) | async-done | bytes 65552 | tf_op jit(solution)/shard_map/psum | solution.py:100
  42.1 1.0 fusion.37
  43.9 6.8 %all-to-all-start = ((bf16[16,16,128]{2,0,1:T(8,128)(2,1)}), bf16[16,16,128]{2,0,1:T(8,128)(2,1)S(1)}, u32[]{:S(2)}, u32[]{:S(2)}) async-start(bf16[16,16,128]{2,0,1:T(8,128)(2,1)} %bitcast.105), calls=%async_computation | async-start | bytes 131072 | tf_op jit(solution)/shard_map/all_to_all | solution.py:135
  51.2 1.2 reshape.240
  52.3 5.9 %all-to-all-done = bf16[16,16,128]{2,0,1:T(8,128)(2,1)S(1)} async-done(((bf16[16,16,128]{2,0,1:T(8,128)(2,1)}), bf16[16,16,128]{2,0,1:T(8,128)(2,1)S(1)}, u32[]{:S(2)}, u32[]{:S(2)}) %all-to-all-start) | async-done | bytes 65568 | tf_op jit(solution)/shard_map/all_to_all | solution.py:135
  58.3 3.7 %all-to-all-start.2 = ((bf16[16,12,2048]{2,1,0:T(8,128)(2,1)}), bf16[16,12,2048]{2,1,0:T(8,128)(2,1)S(1)}, u32[]{:S(2)}, u32[]{:S(2)}) async-start(bf16[16,12,2048]{2,1,0:T(8,128)(2,1)} %reshape.240), calls=%async_computation.4 | async-start | bytes 2097152 | tf_op jit(solution)/shard_map/all_to_all | solution.py:124
  62.0 1.0 fusion.44
  63.2 23.2 %all-to-all-done.2 = bf16[16,12,2048]{2,1,0:T(8,128)(2,1)S(1)} async-done(((bf16[16,12,2048]{2,1,0:T(8,128)(2,1)}), bf16[16,12,2048]{2,1,0:T(8,128)(2,1)S(1)}, u32[]{:S(2)}, u32[]{:S(2)}) %all-to-all-start.2) | async-done | bytes 786464 | tf_op jit(solution)/shard_map/all_to_all | solution.py:124
  86.4 1.7 convolution_bitcast_fusion.2
  88.7 0.8 copy-done.2
  89.5 1.3 fusion.27
  90.8 0.8 convolution_convert_fusion.5
  91.6 0.8 convolution_convert_fusion.6
  92.5 51.5 %reduce-scatter.4.cloned.1.call-done = f32[16,512]{1,0:T(8,128)} async-done(((f32[256,512]{1,0:T(8,128)}), f32[16,512]{1,0:T(8,128)}) %reduce-scatter.4.cloned.1.call-update) | async-done | bytes 32784 | tf_op jit(solution)/shard_map/reduce_scatter | solution.py:137
  144.0 0.7 fusion.52
  144.7 37.0 %all_gather.3 = bf16[256,256]{1,0:T(8,128)(2,1)S(1)} all-gather(bf16[16,256]{1,0:T(8,128)(2,1)S(1)} %fusion.52), channel_id=1, replica_groups=mesh['ep'=16,'tp'=2] {'ep'}, dimensions={0}, use_global_device_ids=true | all-gather | bytes 139264 | tf_op jit(solution)/shard_map/all_gather | solution.py:148
  181.7 0.8 convolution_convert_fusion.3
  182.5 3.5 %all-to-all-start.1 = ((bf16[16,16,128]{2,1,0:T(8,128)(2,1)}), bf16[16,16,128]{2,1,0:T(8,128)(2,1)S(1)}, u32[]{:S(2)}, u32[]{:S(2)}) async-start(bf16[16,16,128]{2,1,0:T(8,128)(2,1)} %bitcast.5), calls=%async_computation.2 | async-start | bytes 131072 | tf_op jit(solution)/shard_map/all_to_all | solution.py:152
  186.5 2.0 copy.64
  188.5 5.0 %all-to-all-done.1 = bf16[16,16,128]{2,1,0:T(8,128)(2,1)S(1)} async-done(((bf16[16,16,128]{2,1,0:T(8,128)(2,1)}), bf16[16,16,128]{2,1,0:T(8,128)(2,1)S(1)}, u32[]{:S(2)}, u32[]{:S(2)}) %all-to-all-start.1) | async-done | bytes 65568 | tf_op jit(solution)/shard_map/all_to_all | solution.py:152
  193.5 3.6 %all-to-all-start.3 = ((bf16[16,12,1024]{2,1,0:T(8,128)(2,1)}), bf16[16,12,1024]{2,1,0:T(8,128)(2,1)S(1)}, u32[]{:S(2)}, u32[]{:S(2)}) async-start(bf16[16,12,1024]{2,1,0:T(8,128)(2,1)} %copy.64), calls=%async_computation.6 | async-start | bytes 1048576 | tf_op jit(solution)/shard_map/all_to_all | solution.py:130
  197.9 9.9 %all-to-all-done.3 = bf16[16,12,1024]{2,1,0:T(8,128)(2,1)S(1)} async-done(((bf16[16,12,1024]{2,1,0:T(8,128)(2,1)}), bf16[16,12,1024]{2,1,0:T(8,128)(2,1)S(1)}, u32[]{:S(2)}, u32[]{:S(2)}) %all-to-all-start.3) | async-done | bytes 393248 | tf_op jit(solution)/shard_map/all_to_all | solution.py:130
  207.9 0.8 gather_fusion
  209.0 1.5 add_convert_fusion
  (78 shorter events, 5.1 us)
Async XLA Ops:
  7.2 9.4 %copy-start = (bf16[512,2048]{1,0:T(8,128)(2,1)S(1)}, bf16[512,2048]{1,0:T(8,128)(2,1)}, u32[]{:S(2)}) copy-start(bf16[512,2048]{1,0:T(8,128)(2,1)} %param.31) | copy-start | bytes 6291460
  7.2 5.3 %copy-start.9 = (s32[16]{0:T(128)S(1)}, s32[16]{0:T(128)}, u32[]{:S(2)}) copy-start(s32[16]{0:T(128)} %param.23) | copy-start | bytes 196
  7.2 5.3 %copy-start.16 = (f32[8]{0:T(128)S(1)}, f32[8]{0:T(128)}, u32[]{:S(2)}) copy-start(f32[8]{0:T(128)} %param.28) | copy-start | bytes 100
  7.2 34.9 %all-reduce.2.cloned.1.call-start = ((), (), s32[]{:S(2)}) async-start(), calls=%async_computation.7 | async-start | bytes 131072 | tf_op jit(solution)/shard_map/psum | solution.py:100
  14.4 1.6 copy-start.1
  16.4 1.2 copy-start.8
  16.4 25.7 %copy-start.3 = (bf16[16,2048]{1,0:T(8,128)(2,1)S(1)}, bf16[16,2048]{1,0:T(8,128)(2,1)}, u32[]{:S(2)}) copy-start(bf16[16,2048]{1,0:T(8,128)(2,1)} %param.22) | copy-start | bytes 196612
  16.4 26.6 %copy-start.7 = (f32[2048]{0:T(1024)S(1)}, f32[2048]{0:T(1024)}, u32[]{:S(2)}) copy-start(f32[2048]{0:T(1024)} %param.32) | copy-start | bytes 24580
  16.4 26.6 %copy-start.11 = (f32[2048]{0:T(1024)S(1)}, f32[2048]{0:T(1024)}, u32[]{:S(2)}) copy-start(f32[2048]{0:T(1024)} %param.38) | copy-start | bytes 24580
  43.9 14.4 %all-to-all-start = ((bf16[16,16,128]{2,0,1:T(8,128)(2,1)}), bf16[16,16,128]{2,0,1:T(8,128)(2,1)S(1)}, u32[]{:S(2)}, u32[]{:S(2)}) async-start(bf16[16,16,128]{2,0,1:T(8,128)(2,1)} %bitcast.105), calls=%async_computation | async-start | bytes 131072 | tf_op jit(solution)/shard_map/all_to_all | solution.py:135
  51.2 10.8 %copy-start.5 = (bf16[128,256]{1,0:T(8,128)(2,1)S(1)}, bf16[128,256]{1,0:T(8,128)(2,1)}, u32[]{:S(2)}) copy-start(bf16[128,256]{1,0:T(8,128)(2,1)} %param.36) | copy-start | bytes 196612
  51.2 10.8 %copy-start.6 = (bf16[128,256]{1,0:T(8,128)(2,1)S(1)}, bf16[128,256]{1,0:T(8,128)(2,1)}, u32[]{:S(2)}) copy-start(bf16[128,256]{1,0:T(8,128)(2,1)} %param.35) | copy-start | bytes 196612
  58.3 28.1 %all-to-all-start.2 = ((bf16[16,12,2048]{2,1,0:T(8,128)(2,1)}), bf16[16,12,2048]{2,1,0:T(8,128)(2,1)S(1)}, u32[]{:S(2)}, u32[]{:S(2)}) async-start(bf16[16,12,2048]{2,1,0:T(8,128)(2,1)} %reshape.240), calls=%async_computation.4 | async-start | bytes 2097152 | tf_op jit(solution)/shard_map/all_to_all | solution.py:124
  62.0 82.0 %reduce-scatter.4.cloned.1.call-start = ((), (), s32[]{:S(2)}) async-start(), calls=%async_computation.8 | async-start | bytes 557056 | tf_op jit(solution)/shard_map/reduce_scatter | solution.py:137
  63.1 123.4 %reduce-scatter.8.cloned.1.call-start = ((), (), s32[]{:S(2)}) async-start(), calls=%async_computation.10 | async-start | bytes 1179648 | tf_op jit(solution)/shard_map/reduce_scatter | solution.py:63
  86.4 1.8 copy-start.12
  88.2 1.2 copy-start.2
  89.4 1.3 copy-start.10
  89.4 1.3 copy-start.13
  89.4 2.2 %copy-start.14 = (bf16[2048,64]{0,1:T(8,128)(2,1)S(1)}, bf16[2048,64]{0,1:T(8,128)(2,1)}, u32[]{:S(2)}) copy-start(bf16[2048,64]{0,1:T(8,128)(2,1)} %param.26) | copy-start | bytes 786436
  89.5 92.3 %copy-start.4 = (bf16[256,128]{1,0:T(8,128)(2,1)S(1)}, bf16[256,128]{1,0:T(8,128)(2,1)}, u32[]{:S(2)}) copy-start(bf16[256,128]{1,0:T(8,128)(2,1)} %param.37) | copy-start | bytes 196612
  89.5 96.5 %copy-start.15 = (bf16[2048,16]{0,1:T(8,128)(2,1)S(1)}, bf16[2048,16]{0,1:T(8,128)(2,1)}, u32[]{:S(2)}) copy-start(bf16[2048,16]{0,1:T(8,128)(2,1)} %param.33) | copy-start | bytes 196612
  182.5 11.0 %all-to-all-start.1 = ((bf16[16,16,128]{2,1,0:T(8,128)(2,1)}), bf16[16,16,128]{2,1,0:T(8,128)(2,1)S(1)}, u32[]{:S(2)}, u32[]{:S(2)}) async-start(bf16[16,16,128]{2,1,0:T(8,128)(2,1)} %bitcast.5), calls=%async_computation.2 | async-start | bytes 131072 | tf_op jit(solution)/shard_map/all_to_all | solution.py:152
  193.5 14.3 %all-to-all-start.3 = ((bf16[16,12,1024]{2,1,0:T(8,128)(2,1)}), bf16[16,12,1024]{2,1,0:T(8,128)(2,1)S(1)}, u32[]{:S(2)}, u32[]{:S(2)}) async-start(bf16[16,12,1024]{2,1,0:T(8,128)(2,1)} %copy.64), calls=%async_computation.6 | async-start | bytes 1048576 | tf_op jit(solution)/shard_map/all_to_all | solution.py:130
  197.1 11.9 %reduce-scatter.6.cloned.1.call-start = ((), (), s32[]{:S(2)}) async-start(), calls=%async_computation.9 | async-start | bytes 98304 | tf_op jit(solution)/shard_map/reduce_scatter | solution.py:155
Sparse Core Ops, SparseCore 0:
  17.7 24.2 all-reduce.1
  65.0 78.8 reduce-scatter.3
  146.2 4.7 reduce-scatter.7
  199.8 8.7 reduce-scatter.5
where the time goes:
time: 218 us; the launch traced here: 217 us
  waiting for transfers between devices  119 us (55%)
  blocking collectives  37 us (17%)
  starting transfers between devices  17.7 us (8%)
  between operations  14.8 us (7%)
  matrix products  13.6 us (6%)
  local copies, waits for them, and re-layouts  7.75 us (4%)
  other arithmetic  6.66 us (3%)
    reduce_scatter x1, waiting for transfers between devices, shards(): lax.psum_scatter(jnp.dot(features2, paired_weights, preferred_element_typ...  51.5 us
    all_gather x1, blocking collectives, shards(): lax.all_gather(dense_hidden, 'ep', axis=0, tiled=True)  37 us
    psum x1, waiting for transfers between devices, shards(): attn = lax.psum(attn_partial, 'tp').astype(jnp.float32)  23.8 us
    all_to_all x1, waiting for transfers between devices, shards(): lax.all_to_all(send_rows, 'ep', split_axis=0, concat_axis=0, tiled=True)  23.2 us
    all_to_all x1, waiting for transfers between devices, shards(): lax.all_to_all(summed, 'ep', split_axis=0, concat_axis=0, tiled=True)  9.93 us
    all_to_all x1, starting transfers between devices, shards(): lax.all_to_all(normed2, 'ep', split_axis=1, concat_axis=0, tiled=True)  6.83 us
    all_to_all x1, waiting for transfers between devices, shards(): lax.all_to_all(normed2, 'ep', split_axis=1, concat_axis=0, tiled=True)  5.95 us
    all_to_all x1, waiting for transfers between devices, shards(): lax.all_to_all(dense_columns.astype(jnp.bfloat16), 'ep', split_axis=0, co...  5.01 us
  transfers between devices with their start and end apart: 8, of which 6 were waited for; matrix products, arithmetic and copies ran while one was open for 7% of the time, Pallas kernels for 0%

commit v1 on v0

--- a/solution.py
+++ b/solution.py
@@ -97,7 +97,7 @@
     attn_partial = jnp.dot(heads_out, w_attn_out, preferred_element_type=jnp.float32).astype(
         jnp.bfloat16
     )
-    attn = lax.psum(attn_partial, "tp").astype(jnp.float32)
+    attn = jnp.sum(lax.all_gather(attn_partial, "tp"), axis=0).astype(jnp.float32)
     residual = (tokens.astype(jnp.float32) + attn).astype(jnp.bfloat16)
     normed2 = rms_scale(residual, ffn_gain).astype(jnp.bfloat16)
     expert_total = w_router.shape[1]

time: 218 us -> 199 us (0.913)
  waiting for transfers between devices: 119 us -> 95 us
  starting transfers between devices: 17.7 us -> 22.9 us
    psum x1 -> x0, waiting for transfers between devices: 23.8 us -> none  [shards(): attn = lax.psum(attn_partial, 'tp').astype(jnp.float32)]
    all_to_all x1, starting transfers between devices: 6.83 us -> 12.1 us  [shards(): lax.all_to_all(normed2, 'ep', split_axis=1, concat_axis=0, tiled=True)]
  transfers between devices with their start and end apart: 8 -> 7, of which waited for: 6 -> 5; matrix products, arithmetic and copies ran while one was open for 7% -> 7% of each run, Pallas kernels for 0% -> 0%
where the time goes in v1:
time: 199 us; the launch traced here: 198 us
  waiting for transfers between devices  95 us (48%)
  blocking collectives  39 us (20%)
  starting transfers between devices  22.9 us (12%)
  between operations  14.8 us (7%)
  matrix products  13 us (7%)
  local copies, waits for them, and re-layouts  7.75 us (4%)
  other arithmetic  5.84 us (3%)
    reduce_scatter x1, waiting for transfers between devices, shards(): lax.psum_scatter(jnp.dot(features2, paired_weights, preferred_element_typ...  51.7 us
    all_gather x1, blocking collectives, shards(): lax.all_gather(dense_hidden, 'ep', axis=0, tiled=True)  37 us
    all_to_all x1, waiting for transfers between devices, shards(): lax.all_to_all(send_rows, 'ep', split_axis=0, concat_axis=0, tiled=True)  23.3 us
    all_to_all x1, starting transfers between devices, shards(): lax.all_to_all(normed2, 'ep', split_axis=1, concat_axis=0, tiled=True)  12.1 us
    all_to_all x1, waiting for transfers between devices, shards(): lax.all_to_all(summed, 'ep', split_axis=0, concat_axis=0, tiled=True)  9.1 us
    all_to_all x1, waiting for transfers between devices, shards(): lax.all_to_all(dense_columns.astype(jnp.bfloat16), 'ep', split_axis=0, co...  5.43 us
    all_to_all x1, waiting for transfers between devices, shards(): lax.all_to_all(normed2, 'ep', split_axis=1, concat_axis=0, tiled=True)  5.28 us
  transfers between devices with their start and end apart: 7, of which 5 were waited for; matrix products, arithmetic and copies ran while one was open for 7% of the time, Pallas kernels for 0%

profile of v1, /device:TPU:0, one launch (start us, length us, event | category | flops | bytes accessed | tf_op | source)
XLA Modules:
  0.0 198.3 jit_solution(2389787002278691970)
XLA Ops:
  7.2 1.4 reduce_max.9
  9.3 1.0 fusion.40
  10.3 2.1 %convolution_convert_fusion.4 = bf16[16,512]{1,0:T(8,128)(2,1)S(1)} fusion(bf16[2048,512]{1,0:T(8,128)(2,1)} %param.25, bf16[16,2048]{1,0:T(8,128)(2,1)} %param.22, f32[2048]{0:T(1024)} %param.24, f32[16]{0:T(128)S(1)} %add_rsqrt_fusion.1), kind=kOutput, calls=%fused_computation.44 | convolution fusion | flops 33693696 | bytes 2187328 | tf_op jit(solution)/shard_map/dot_general | solution.py:95
  12.5 3.9 %while.15 = (s32[]{:T(128)}, f32[16,1,8,64]{3,2,0,1:T(8,128)S(1)}, f32[16,1,8]{0,2,1:T(8,128)S(1)}, s32[]{:T(128)}, s32[]{:T(128)}, /*index=5*/s32[16]{0:T(128)S...) while((s32[]{:T(128)}, f32[16,1,8,64]{3,2,0,1:T(8,128)S(1)}, ...), condition=%wide.region_4.5_spmd.clone, body=%wide.region_2.4_spmd.clone.sunk | while | flops 422003200 | bytes 11420487 | solution.py:49
  12.6 1.6 fusion.88
  14.3 0.9 fusion.89
  15.3 0.7 copy-done.1
  16.9 2.0 %all-gather = bf16[32,2048]{1,0:T(8,128)(2,1)S(1)} all-gather(bf16[16,2048]{1,0:T(8,128)(2,1)S(1)} %convolution_convert_fusion.2), channel_id=2, replica_groups=mesh['ep'=16,'tp'=2] {'tp'}, dimensions={0}, use_global_device_ids=true | all-gather | bytes 196608 | tf_op jit(solution)/shard_map/all_gather | solution.py:100
  19.4 0.6 copy.80
  20.0 12.1 %all-to-all-start = ((bf16[16,16,128]{2,0,1:T(8,128)(2,1)}), bf16[16,16,128]{2,0,1:T(8,128)(2,1)S(1)}, u32[]{:S(2)}, u32[]{:S(2)}) async-start(bf16[16,16,128]{2,0,1:T(8,128)(2,1)} %bitcast.106), calls=%async_computation | async-start | bytes 131072 | tf_op jit(solution)/shard_map/all_to_all | solution.py:135
  33.2 1.2 reshape.240
  34.3 5.3 %all-to-all-done = bf16[16,16,128]{2,0,1:T(8,128)(2,1)S(1)} async-done(((bf16[16,16,128]{2,0,1:T(8,128)(2,1)}), bf16[16,16,128]{2,0,1:T(8,128)(2,1)S(1)}, u32[]{:S(2)}, u32[]{:S(2)}) %all-to-all-start) | async-done | bytes 65568 | tf_op jit(solution)/shard_map/all_to_all | solution.py:135
  39.6 3.7 %all-to-all-start.2 = ((bf16[16,12,2048]{2,1,0:T(8,128)(2,1)}), bf16[16,12,2048]{2,1,0:T(8,128)(2,1)S(1)}, u32[]{:S(2)}, u32[]{:S(2)}) async-start(bf16[16,12,2048]{2,1,0:T(8,128)(2,1)} %reshape.240), calls=%async_computation.4 | async-start | bytes 2097152 | tf_op jit(solution)/shard_map/all_to_all | solution.py:124
  43.3 1.0 fusion.44
  44.4 23.3 %all-to-all-done.2 = bf16[16,12,2048]{2,1,0:T(8,128)(2,1)S(1)} async-done(((bf16[16,12,2048]{2,1,0:T(8,128)(2,1)}), bf16[16,12,2048]{2,1,0:T(8,128)(2,1)S(1)}, u32[]{:S(2)}, u32[]{:S(2)}) %all-to-all-start.2) | async-done | bytes 786464 | tf_op jit(solution)/shard_map/all_to_all | solution.py:124
  67.8 1.8 convolution_bitcast_fusion.2
  70.0 0.8 copy-done.2
  70.8 1.3 fusion.27
  72.7 0.8 convolution_convert_fusion.5
  73.5 51.7 %reduce-scatter.4.cloned.1.call-done = f32[16,512]{1,0:T(8,128)} async-done(((f32[256,512]{1,0:T(8,128)}), f32[16,512]{1,0:T(8,128)}) %reduce-scatter.4.cloned.1.call-update) | async-done | bytes 32784 | tf_op jit(solution)/shard_map/reduce_scatter | solution.py:137
  125.2 0.7 fusion.52
  126.0 37.0 %all_gather.11 = bf16[256,256]{1,0:T(8,128)(2,1)S(1)} all-gather(bf16[16,256]{1,0:T(8,128)(2,1)S(1)} %fusion.52), channel_id=1, replica_groups=mesh['ep'=16,'tp'=2] {'ep'}, dimensions={0}, use_global_device_ids=true | all-gather | bytes 139264 | tf_op jit(solution)/shard_map/all_gather | solution.py:148
  163.0 0.8 convolution_convert_fusion.3
  163.8 3.5 %all-to-all-start.1 = ((bf16[16,16,128]{2,1,0:T(8,128)(2,1)}), bf16[16,16,128]{2,1,0:T(8,128)(2,1)S(1)}, u32[]{:S(2)}, u32[]{:S(2)}) async-start(bf16[16,16,128]{2,1,0:T(8,128)(2,1)} %bitcast.6), calls=%async_computation.2 | async-start | bytes 131072 | tf_op jit(solution)/shard_map/all_to_all | solution.py:152
  167.3 2.0 %copy.73 = bf16[16,12,1024]{2,1,0:T(8,128)(2,1)} copy(bf16[16,12,1024]{2,0,1:T(8,128)(2,1)} %bitcast.128) | data formatting | bytes 786432 | tf_op jit(solution)/shard_map/reshape | solution.py:129
  169.4 5.4 %all-to-all-done.1 = bf16[16,16,128]{2,1,0:T(8,128)(2,1)S(1)} async-done(((bf16[16,16,128]{2,1,0:T(8,128)(2,1)}), bf16[16,16,128]{2,1,0:T(8,128)(2,1)S(1)}, u32[]{:S(2)}, u32[]{:S(2)}) %all-to-all-start.1) | async-done | bytes 65568 | tf_op jit(solution)/shard_map/all_to_all | solution.py:152
  174.8 3.6 %all-to-all-start.3 = ((bf16[16,12,1024]{2,1,0:T(8,128)(2,1)}), bf16[16,12,1024]{2,1,0:T(8,128)(2,1)S(1)}, u32[]{:S(2)}, u32[]{:S(2)}) async-start(bf16[16,12,1024]{2,1,0:T(8,128)(2,1)} %copy.73), calls=%async_computation.6 | async-start | bytes 1048576 | tf_op jit(solution)/shard_map/all_to_all | solution.py:130
  178.5 0.8 convolution_convert_fusion.6
  179.4 0.6 copy_bitcast_fusion
  180.0 9.1 %all-to-all-done.3 = bf16[16,12,1024]{2,1,0:T(8,128)(2,1)S(1)} async-done(((bf16[16,12,1024]{2,1,0:T(8,128)(2,1)}), bf16[16,12,1024]{2,1,0:T(8,128)(2,1)S(1)}, u32[]{:S(2)}, u32[]{:S(2)}) %all-to-all-start.3) | async-done | bytes 393248 | tf_op jit(solution)/shard_map/all_to_all | solution.py:130
  189.2 0.8 gather_fusion
  190.3 1.5 add_convert_fusion
  (77 shorter events, 4.4 us)
Async XLA Ops:
  7.2 9.4 %copy-start = (bf16[512,2048]{1,0:T(8,128)(2,1)S(1)}, bf16[512,2048]{1,0:T(8,128)(2,1)}, u32[]{:S(2)}) copy-start(bf16[512,2048]{1,0:T(8,128)(2,1)} %param.31) | copy-start | bytes 6291460
  7.2 5.3 %copy-start.9 = (s32[16]{0:T(128)S(1)}, s32[16]{0:T(128)}, u32[]{:S(2)}) copy-start(s32[16]{0:T(128)} %param.23) | copy-start | bytes 196
  7.2 5.3 %copy-start.16 = (f32[8]{0:T(128)S(1)}, f32[8]{0:T(128)}, u32[]{:S(2)}) copy-start(f32[8]{0:T(128)} %param.28) | copy-start | bytes 100
  14.3 1.6 copy-start.1
  16.4 2.6 %copy-start.3 = (bf16[16,2048]{1,0:T(8,128)(2,1)S(1)}, bf16[16,2048]{1,0:T(8,128)(2,1)}, u32[]{:S(2)}) copy-start(bf16[16,2048]{1,0:T(8,128)(2,1)} %param.22) | copy-start | bytes 196612
  16.4 2.8 %copy-start.7 = (f32[2048]{0:T(1024)S(1)}, f32[2048]{0:T(1024)}, u32[]{:S(2)}) copy-start(f32[2048]{0:T(1024)} %param.32) | copy-start | bytes 24580
  16.4 2.8 %copy-start.11 = (f32[2048]{0:T(1024)S(1)}, f32[2048]{0:T(1024)}, u32[]{:S(2)}) copy-start(f32[2048]{0:T(1024)} %param.38) | copy-start | bytes 24580
  16.4 15.7 %copy-start.8 = (s32[16,6]{0,1:T(8,128)S(1)}, s32[16,6]{0,1:T(8,128)}, u32[]{:S(2)}) copy-start(s32[16,6]{0,1:T(8,128)} %param.34) | copy-start | bytes 1156
  20.0 19.6 %all-to-all-start = ((bf16[16,16,128]{2,0,1:T(8,128)(2,1)}), bf16[16,16,128]{2,0,1:T(8,128)(2,1)S(1)}, u32[]{:S(2)}, u32[]{:S(2)}) async-start(bf16[16,16,128]{2,0,1:T(8,128)(2,1)} %bitcast.106), calls=%async_computation | async-start | bytes 131072 | tf_op jit(solution)/shard_map/all_to_all | solution.py:135
  33.1 10.2 %copy-start.5 = (bf16[128,256]{1,0:T(8,128)(2,1)S(1)}, bf16[128,256]{1,0:T(8,128)(2,1)}, u32[]{:S(2)}) copy-start(bf16[128,256]{1,0:T(8,128)(2,1)} %param.36) | copy-start | bytes 196612
  33.2 10.2 %copy-start.6 = (bf16[128,256]{1,0:T(8,128)(2,1)S(1)}, bf16[128,256]{1,0:T(8,128)(2,1)}, u32[]{:S(2)}) copy-start(bf16[128,256]{1,0:T(8,128)(2,1)} %param.35) | copy-start | bytes 196612
  39.6 28.2 %all-to-all-start.2 = ((bf16[16,12,2048]{2,1,0:T(8,128)(2,1)}), bf16[16,12,2048]{2,1,0:T(8,128)(2,1)S(1)}, u32[]{:S(2)}, u32[]{:S(2)}) async-start(bf16[16,12,2048]{2,1,0:T(8,128)(2,1)} %reshape.240), calls=%async_computation.4 | async-start | bytes 2097152 | tf_op jit(solution)/shard_map/all_to_all | solution.py:124
  43.3 82.0 %reduce-scatter.4.cloned.1.call-start = ((), (), s32[]{:S(2)}) async-start(), calls=%async_computation.7 | async-start | bytes 557056 | tf_op jit(solution)/shard_map/reduce_scatter | solution.py:137
  44.4 122.9 %reduce-scatter.8.cloned.1.call-start = ((), (), s32[]{:S(2)}) async-start(), calls=%async_computation.9 | async-start | bytes 1179648 | tf_op jit(solution)/shard_map/reduce_scatter | solution.py:63
  67.8 1.8 copy-start.12
  69.5 1.2 copy-start.2
  70.8 1.3 copy-start.15
  70.8 1.9 copy-start.10
  70.8 1.9 copy-start.13
  70.8 92.2 %copy-start.4 = (bf16[256,128]{1,0:T(8,128)(2,1)S(1)}, bf16[256,128]{1,0:T(8,128)(2,1)}, u32[]{:S(2)}) copy-start(bf16[256,128]{1,0:T(8,128)(2,1)} %param.37) | copy-start | bytes 196612
  72.1 106.5 %copy-start.14 = (bf16[2048,64]{0,1:T(8,128)(2,1)S(1)}, bf16[2048,64]{0,1:T(8,128)(2,1)}, u32[]{:S(2)}) copy-start(bf16[2048,64]{0,1:T(8,128)(2,1)} %param.26) | copy-start | bytes 786436
  163.8 11.0 %all-to-all-start.1 = ((bf16[16,16,128]{2,1,0:T(8,128)(2,1)}), bf16[16,16,128]{2,1,0:T(8,128)(2,1)S(1)}, u32[]{:S(2)}, u32[]{:S(2)}) async-start(bf16[16,16,128]{2,1,0:T(8,128)(2,1)} %bitcast.6), calls=%async_computation.2 | async-start | bytes 131072 | tf_op jit(solution)/shard_map/all_to_all | solution.py:152
  174.8 14.3 %all-to-all-start.3 = ((bf16[16,12,1024]{2,1,0:T(8,128)(2,1)}), bf16[16,12,1024]{2,1,0:T(8,128)(2,1)S(1)}, u32[]{:S(2)}, u32[]{:S(2)}) async-start(bf16[16,12,1024]{2,1,0:T(8,128)(2,1)} %copy.73), calls=%async_computation.6 | async-start | bytes 1048576 | tf_op jit(solution)/shard_map/all_to_all | solution.py:130
  178.4 11.9 %reduce-scatter.6.cloned.1.call-start = ((), (), s32[]{:S(2)}) async-start(), calls=%async_computation.8 | async-start | bytes 98304 | tf_op jit(solution)/shard_map/reduce_scatter | solution.py:155
Sparse Core Ops, SparseCore 0:
  46.3 78.8 reduce-scatter.3
  127.5 4.7 reduce-scatter.7
  181.4 8.7 reduce-scatter.5
